TPU v7x, 32 devices: a whole 2x2x4 slice. The times are simulated.
32 devices in a mesh: fs: 8 (over z, y), tp: 4 (over x, core).
Axes of the slice: x: 2, y: 2, z: 4, core: 2. Of those that a mesh axis runs over, the one named last changes fastest.
Arguments:
- tokens: bfloat16 [4096, 2048], P(('fs', 'tp')), may hold values from -6 to 6
- pre_gain: float32 [2048], replicated, may hold values from 0.1 to 1.9
- w_expand: bfloat16 [2048, 8192], P('fs', 'tp'), may hold values from -0.125 to 0.125
- w_reduce: bfloat16 [8192, 2048], P('tp', 'fs'), may hold values from -0.0625 to 0.0625
- post_gain: float32 [2048], replicated, may hold values from 0.1 to 1.9
Outputs:
- result: bfloat16 [4096, 2048], P(('fs', 'tp'))
All inputs are finite; a program needn't handle non-finite values.
Results may differ from a plain program's by a relative error of at most 0.014.
Values may be sent and summed in bfloat16 or wider, within the bound.
A program may use at most 64 MiB of HBM per device.

v0:
```python
import jax
import jax.numpy as jnp
from jax import lax
from jax.sharding import PartitionSpec as P

NORM_EPS = 1e-06


def rms_scale(values, gain_row):
    widened = values.astype(jnp.float32)
    scaled = widened * lax.rsqrt(jnp.mean(widened * widened, axis=-1, keepdims=True) + NORM_EPS)
    return scaled * gain_row


def squared_relu(preact):
    return jnp.square(jnp.maximum(preact, 0.0)).astype(jnp.bfloat16)


def per_device(tokens, pre_gain, w_expand, w_reduce, post_gain):
    normed = rms_scale(tokens, pre_gain).astype(jnp.bfloat16)
    expand_full = lax.all_gather(w_expand, "fs", axis=0, tiled=True)
    hidden = squared_relu(
        jnp.dot(
            lax.all_gather(normed, "tp", axis=0, tiled=True),
            expand_full,
            preferred_element_type=jnp.float32,
        )
    )
    reduce_full = lax.all_gather(w_reduce, "fs", axis=1, tiled=True)
    mixed = lax.psum_scatter(
        jnp.dot(hidden, reduce_full, preferred_element_type=jnp.float32).astype(jnp.bfloat16),
        "tp",
        scatter_dimension=0,
        tiled=True,
    )
    return rms_scale(mixed, post_gain).astype(jnp.bfloat16)


def solution(mesh):
    return jax.shard_map(
        per_device,
        mesh=mesh,
        in_specs=(P(("fs", "tp"), None), P(), P("fs", "tp"), P("tp", "fs"), P()),
        out_specs=P(("fs", "tp"), None),
        check_vma=False,
    )
```

profile of v0, /device:TPU:1, one launch (start us, length us, event | category | flops | bytes accessed | tf_op | source)
XLA Modules:
  0.0 342.1 jit_solution(1764702396853761959)
XLA Ops:
  6.5 0.0 all-gather.4.cloned.1.call-start
  6.5 1.2 fusion
  7.8 2.0 fusion.2
  9.8 0.0 all-gather.4.cloned.1.call-update
  9.8 0.0 all-gather.6.cloned.1.call-start
  9.9 0.7 all-gather.6.cloned.1.call-update
  10.6 0.0 all-gather.8.cloned.1.call-start
  10.6 0.7 all-gather.8.cloned.1.call-update
  11.3 0.0 copy-start
  11.3 0.0 reduce-scatter.2.cloned.1.call-start
  11.4 23.6 %all-gather.4.cloned.1.call-done = bf16[512,2048]{1,0:T(8,128)(2,1)} async-done(((bf16[128,2048]{1,0:T(8,128)(2,1)}), bf16[512,2048]{1,0:T(8,128)(2,1)}) %all-gather.4.cloned.1.call-update) | async-done | bytes 2097168 | tf_op jit(solution)/shard_map/all_gather | solution.py:24
  35.0 125.5 %all-gather.6.cloned.1.call-done = bf16[2048,2048]{1,0:T(8,128)(2,1)} async-done(((bf16[256,2048]{1,0:T(8,128)(2,1)}), bf16[2048,2048]{1,0:T(8,128)(2,1)}) %all-gather.6.cloned.1.call-update) | async-done | bytes 8388624 | tf_op jit(solution)/shard_map/all_gather | solution.py:21
  160.5 125.1 %all-gather.8.cloned.1.call-done = bf16[2048,2048]{1,0:T(8,128)(2,1)} async-done(((bf16[2048,256]{1,0:T(8,128)(2,1)}), bf16[2048,2048]{1,0:T(8,128)(2,1)}) %all-gather.8.cloned.1.call-update) | async-done | bytes 8388624 | tf_op jit(solution)/shard_map/all_gather | solution.py:29
  285.7 16.5 %convolution_convert_fusion = bf16[512,2048]{1,0:T(8,128)(2,1)} fusion(bf16[2048,2048]{1,0:T(8,128)(2,1)} %all-gather.8.cloned.1.call-done, bf16[512,2048]{1,0:T(8,128)(2,1)} %all-gather.4.cloned.1.call-done, bf16[2048,2048]{1,0:T(8,128)(2,1)} %all-gather.6.cloned.1.call-done), kind=kOutput, calls=%fused_computation.1 | convolution fusion | flops 8594128896 | bytes 20971520 | tf_op jit(solution)/shard_map/dot_general | solution.py:31
  302.2 0.0 reduce-scatter.2.cloned.1.call-update
  302.2 30.1 %reduce-scatter.2.cloned.1.call-done = bf16[128,2048]{1,0:T(8,128)(2,1)} async-done(((bf16[512,2048]{1,0:T(8,128)(2,1)}), bf16[128,2048]{1,0:T(8,128)(2,1)}) %reduce-scatter.2.cloned.1.call-update) | async-done | bytes 524304 | tf_op jit(solution)/shard_map/reduce_scatter | solution.py:30
  332.3 1.2 fusion.3
  333.6 0.0 copy-done
  333.6 2.0 fusion.5
  (2 shorter events, 0.0 us)
Async XLA Ops:
  6.5 28.5 %all-gather.4.cloned.1.call-start = ((), (), s32[]{:S(2)}) async-start(), calls=%async_computation.1 | async-start | bytes 2621440 | tf_op jit(solution)/shard_map/all_gather | solution.py:24
  9.8 150.7 %all-gather.6.cloned.1.call-start = ((), (), s32[]{:S(2)}) async-start(), calls=%async_computation.2 | async-start | bytes 9437184 | tf_op jit(solution)/shard_map/all_gather | solution.py:21
  10.6 275.1 %all-gather.8.cloned.1.call-start = ((), (), s32[]{:S(2)}) async-start(), calls=%async_computation.3 | async-start | bytes 9437184 | tf_op jit(solution)/shard_map/all_gather | solution.py:29
  11.3 322.2 %copy-start = (f32[2048]{0:T(1024)S(1)}, f32[2048]{0:T(1024)}, u32[]{:S(2)}) copy-start(f32[2048]{0:T(1024)} %param.9) | copy-start | bytes 24580
  11.3 321.0 %reduce-scatter.2.cloned.1.call-start = ((), (), s32[]{:S(2)}) async-start(), calls=%async_computation.4 | async-start | bytes 2621440 | tf_op jit(solution)/shard_map/reduce_scatter | solution.py:30
Sparse Core Ops, SparseCore 0:
  9.9 25.0 all-gather.3
  37.1 123.3 all-gather.5
  162.6 123.0 all-gather.7
  302.3 29.9 reduce-scatter.1
where the time goes:
time: 343 us; the launch traced here: 342 us
  waiting for transfers between devices  306 us (89%)
  matrix products  16.5 us (5%)
  between operations  13.1 us (4%)
  other arithmetic  6.53 us (2%)
    all_gather x1, waiting for transfers between devices, per_device(): expand_full = lax.all_gather(w_expand, 'fs', axis=0, tiled=True)  126 us
    all_gather x1, waiting for transfers between devices, per_device(): reduce_full = lax.all_gather(w_reduce, 'fs', axis=1, tiled=True)  125 us
    reduce_scatter x1, waiting for transfers between devices, per_device(): lax.psum_scatter(jnp.dot(hidden, reduce_full, preferred_element_type=jnp....  30.1 us
    all_gather x1, waiting for transfers between devices, per_device(): lax.all_gather(normed, 'tp', axis=0, tiled=True)  23.6 us
    dot_general x1, matrix products, per_device(): jnp.dot(hidden, reduce_full, preferred_element_type=jnp.float32)  16.5 us
  transfers between devices with their start and end apart: 4, of which 4 were waited for; matrix products, arithmetic and copies ran while one was open for 0% of the time, Pallas kernels for 0%

commit v1 on v0

v1 whole, which is shorter than its diff:
```python
import functools
import math

import jax
import jax.numpy as jnp
from jax import lax
from jax.experimental import pallas as pl
from jax.experimental.pallas import tpu as pltpu
from jax.sharding import PartitionSpec as P

NORM_EPS = 1e-06
MESH = pl.DeviceIdType.MESH


def kernel(NX, NY, NZ, tok, gain_in, w_e, w_r, gain_out, out,
           TG, N, WE, WR, H, O, PR, RX,
           t_ls, t_ps, t_r, e_a, e_b, e_c, e_r, r_a, r_b, r_c, r_r, p_s, p_r, c_s, c_r):
    R, D = tok.shape
    DK, F = w_e.shape
    H4 = F // NZ
    fs, tp = lax.axis_index("fs"), lax.axis_index("tp")
    z, y = fs // NY, fs % NY
    x, c = tp // 2, tp % 2
    pc = 1 - c
    peer = (fs, x * 2 + pc)

    def zdev(q):
        return (q * NY + y, tp)

    xs = [(x + j) % NX for j in range(1, NX)]
    ys = [(y + j) % NY for j in range(1, NY)]
    xdevs = [(fs, q * 2 + c) for q in xs]
    ydevs = [(z * NY + q, tp) for q in ys]

    barrier = pltpu.get_barrier_semaphore()
    others = [zdev((z + j) % NZ) for j in range(1, NZ)] + xdevs + ydevs + [peer]
    for dev in others:
        pl.semaphore_signal(barrier, inc=1, device_id=dev, device_id_type=MESH)
    pl.semaphore_wait(barrier, len(others))

    def rc(src, dst, ss, rs, dev):
        return pltpu.make_async_remote_copy(src_ref=src, dst_ref=dst, send_sem=ss, recv_sem=rs,
                                            device_id=dev, device_id_type=MESH)

    sent = []

    def go(cond, make):
        if cond is None:
            make().start()
        else:
            pl.when(cond)(lambda: make().start())
        sent.append((cond, make))

    def guarded(cond, fn):
        if cond is None:
            fn()
        else:
            pl.when(cond)(fn)

    def at_distance(d):
        if d == 0:
            return [(z, 0, None)]
        return [(z - d, -1, z - d >= 0), (z + d, 1, z + d < NZ)]

    def e_view(xq, zq, yq):
        return WE.at[xq, pl.ds(pl.multiple_of((zq * NY + yq) * DK, DK), DK)]

    def r_view(xq, zq, yq):
        return WR.at[zq * NY + yq, pl.ds(pl.multiple_of(xq * H4, H4), H4)]

    def e_piece(q):
        return w_e.at[:, pl.ds(pl.multiple_of(q * H4, H4), H4)]

    def r_piece(q):
        return w_r.at[pl.ds(pl.multiple_of(q * H4, H4), H4)]

    own = [
        pltpu.make_async_copy(tok, TG.at[z, c], t_r.at[z, c]),
        pltpu.make_async_copy(e_piece(z), e_view(x, z, y), e_r.at[x, z, y]),
        pltpu.make_async_copy(r_piece(z), r_view(x, z, y), r_r.at[x, z, y]),
    ]
    for copy in own:
        copy.start()
    for side, (q, ok) in enumerate(((z - 1, z >= 1), (z + 1, z + 1 < NZ))):
        go(ok, lambda q=q, side=side: rc(tok, TG.at[z, c], t_ls.at[z, side], t_r.at[z, c], zdev(q)))
    go(None, lambda: rc(tok, TG.at[z, c], t_ps.at[z], t_r.at[z, c], peer))
    for view, piece, a_s, r in ((e_view, e_piece, e_a, e_r), (r_view, r_piece, r_a, r_r)):
        for d in range(1, NZ):
            for q, s, ok in at_distance(d):
                go(ok, lambda q=q, view=view, piece=piece, a_s=a_s, r=r:
                   rc(piece(q), view(x, z, y), a_s.at[q], r.at[x, z, y], zdev(q)))

    def landed(ref, sem):
        pltpu.make_async_copy(ref, ref, sem).wait()

    def tokens_step(d):
        for q, s, ok in at_distance(d):
            guarded(ok, lambda q=q: landed(TG.at[q, c], t_r.at[q, c]))
            if d > 0:
                n = z - s
                go(jnp.logical_and(ok, jnp.logical_and(n >= 0, n < NZ)),
                   lambda q=q, n=n, s=s: rc(TG.at[q, c], TG.at[q, c], t_ls.at[q, (1 - s) // 2],
                                            t_r.at[q, c], zdev(n)))
                go(ok, lambda q=q: rc(TG.at[q, c], TG.at[q, c], t_ps.at[q], t_r.at[q, c], peer))

    def first_step(d, view, r, b_s, c_s_, x_first):
        for q, s, ok in at_distance(d):
            guarded(ok, lambda q=q: landed(view(x, q, y), r.at[x, q, y]))
            firsts, lasts = (xdevs, ydevs) if x_first else (ydevs, xdevs)
            for j, dev in enumerate(firsts):
                go(ok, lambda q=q, j=j, dev=dev: rc(view(x, q, y), view(x, q, y), b_s.at[q, j],
                                                    r.at[x, q, y], dev))
            for j, dev in enumerate(lasts):
                go(ok, lambda q=q, j=j, dev=dev: rc(view(x, q, y), view(x, q, y), c_s_.at[q, 0, j],
                                                    r.at[x, q, y], dev))

    def second_step(d, view, r, c_s_, x_first):
        for q, s, ok in at_distance(d):
            for i, m in enumerate(xs if x_first else ys):
                where = (m, q, y) if x_first else (x, q, m)
                guarded(ok, lambda where=where: landed(view(*where), r.at[where]))
                for j, dev in enumerate(ydevs if x_first else xdevs):
                    go(ok, lambda q=q, i=i, j=j, dev=dev, where=where:
                       rc(view(*where), view(*where), c_s_.at[q, 1 + i, j], r.at[where], dev))

    def last_step(d, view, r, x_first):
        for q, s, ok in at_distance(d):
            for a in [x] + xs if x_first else xs:
                for b in ys if x_first else [y] + ys:
                    guarded(ok, lambda q=q, a=a, b=b: landed(view(a, q, b), r.at[a, q, b]))

    def normalize():
        for q in range(NZ):
            landed(TG.at[q, pc], t_r.at[q, pc])
        sub = 32

        def body(i, carry):
            b, row = i // (R // sub), (i % (R // sub)) * sub
            row = pl.multiple_of(row, sub)
            v = TG[b // 2, b % 2, pl.ds(row, sub)].astype(jnp.float32)
            v = v * lax.rsqrt(jnp.mean(v * v, axis=-1, keepdims=True) + NORM_EPS) * gain_in[...]
            N[pl.ds(pl.multiple_of(i * sub, sub), sub)] = v.astype(jnp.bfloat16)
            return carry

        lax.fori_loop(0, NZ * 2 * R // sub, body, 0)

    rows = NZ * 2 * R
    MB = math.gcd(4, NZ * 2)
    M = MB * R

    def expand():
        def body(i, carry):
            xq, row = i // (rows // M), pl.multiple_of((i % (rows // M)) * M, M)
            p = jnp.dot(N[pl.ds(row, M)], WE[xq], preferred_element_type=jnp.float32)
            H[xq, pl.ds(row, M)] = jnp.square(jnp.maximum(p, 0.0)).astype(jnp.bfloat16)
            return carry

        lax.fori_loop(0, NX * (rows // M), body, 0)

    def reduce_column(f):
        def body(i, carry):
            row = pl.multiple_of(i * M, M)
            p = jnp.dot(H[0, pl.ds(row, M)], WR[f, :H4], preferred_element_type=jnp.float32)
            for xq in range(1, NX):
                p += jnp.dot(H[xq, pl.ds(row, M)], WR[f, xq * H4:(xq + 1) * H4],
                             preferred_element_type=jnp.float32)
            O[pl.ds(i * MB, MB), f] = p.astype(jnp.bfloat16).reshape(MB, R, DK)
            return carry

        lax.fori_loop(0, rows // M, body, 0)

    for d in range(NZ):
        tokens_step(d)
        first_step(d, e_view, e_r, e_b, e_c, True)
        if d > 0:
            second_step(d - 1, e_view, e_r, e_c, True)
    second_step(NZ - 1, e_view, e_r, e_c, True)
    for d in range(NZ):
        first_step(d, r_view, r_r, r_b, r_c, False)
        if d > 0:
            second_step(d - 1, r_view, r_r, r_c, False)
        if d == NZ - 2:
            normalize()
            for k in range(NZ):
                last_step(k, e_view, e_r, True)
            expand()
    second_step(NZ - 1, r_view, r_r, r_c, False)
    for d in range(NZ):
        last_step(d, r_view, r_r, False)
    lax.fori_loop(0, NZ * NY, lambda f, carry: (reduce_column(f), carry)[1], 0)

    for k in range(NZ):
        go(None, lambda k=k: rc(O.at[k * 2 + pc], PR.at[k], p_s.at[k], p_r.at[k], peer))

    def add_block(q, slots):
        def body(f, carry):
            s = O[q * 2 + c, f].astype(jnp.float32) + PR[q, f].astype(jnp.float32)
            for slot in slots:
                s += RX[slot, f].astype(jnp.float32)
            O[q * 2 + c, f] = s.astype(jnp.bfloat16)
            return carry

        lax.fori_loop(0, NZ * NY, body, 0)

    for k in range(NZ):
        landed(PR.at[k], p_r.at[k])

    for j in range(NZ - 1):
        for q, n, ok, has in ((NZ - 1 - j, z + 1, NZ - 1 - j > z, z > 0), (j, z - 1, j < z, z < NZ - 1)):
            inner = jnp.logical_and(ok, has)

            def with_arrived(q=q):
                landed(RX.at[q], c_r.at[q])
                add_block(q, [q])

            pl.when(inner)(with_arrived)
            pl.when(jnp.logical_and(ok, jnp.logical_not(has)))(lambda q=q: add_block(q, []))
            slot = jnp.where(jnp.logical_and(n < z, n == q), NZ, q)
            go(ok, lambda q=q, n=n, slot=slot: rc(O.at[q * 2 + c], RX.at[slot], c_s.at[q], c_r.at[slot], zdev(n)))

    pl.when(z > 0)(lambda: landed(RX.at[z], c_r.at[z]))
    pl.when(z < NZ - 1)(lambda: landed(RX.at[NZ], c_r.at[NZ]))
    pl.when(jnp.logical_and(z > 0, z < NZ - 1))(lambda: add_block(z, [z, NZ]))
    pl.when(z == 0)(lambda: add_block(z, [NZ]))
    pl.when(z == NZ - 1)(lambda: add_block(z, [z]))

    def squares(f, acc):
        m = O[z * 2 + c, f].astype(jnp.float32)
        return acc + jnp.sum(m * m, axis=-1, keepdims=True)

    total = lax.fori_loop(0, NZ * NY, squares, jnp.zeros((R, 1), jnp.float32))
    scale = lax.rsqrt(total / D + NORM_EPS)
    for f in range(NZ * NY):
        cols = slice(f * DK, (f + 1) * DK)
        out[:, cols] = (O[z * 2 + c, f].astype(jnp.float32) * scale * gain_out[:, cols]).astype(jnp.bfloat16)

    for cond, make in sent:
        guarded(cond, lambda make=make: make().wait_send())


def per_device(FS, TP, tokens, pre_gain, w_expand, w_reduce, post_gain):
    NX = TP // 2
    NY = max(k for k in range(1, FS + 1) if FS % k == 0 and (k == 1 or 2 * k * k <= FS))
    NZ = FS // NY
    R, D = tokens.shape
    DK, F = w_expand.shape
    H4 = F // NZ
    rows = NZ * 2 * R
    bf = jnp.bfloat16
    dma = pltpu.SemaphoreType.DMA
    mx = max(NX, NY)
    vmem = pl.BlockSpec(memory_space=pltpu.VMEM)
    hbm = pl.BlockSpec(memory_space=pl.ANY)
    return pl.pallas_call(
        functools.partial(kernel, NX, NY, NZ),
        out_shape=jax.ShapeDtypeStruct((R, D), bf),
        in_specs=[hbm, vmem, hbm, hbm, vmem],
        out_specs=vmem,
        scratch_shapes=[
            pltpu.VMEM((NZ, 2, R, D), bf),
            pltpu.VMEM((rows, D), bf),
            pltpu.VMEM((NX, D, H4), bf),
            pltpu.VMEM((FS, NX * H4, DK), bf),
            pltpu.VMEM((NX, rows, H4), bf),
            pltpu.VMEM((NZ * 2, FS, R, DK), bf),
            pltpu.VMEM((NZ, FS, R, DK), bf),
            pltpu.VMEM((NZ + 1, FS, R, DK), bf),
            dma((NZ, 2)), dma((NZ,)), dma((NZ, 2)),
            dma((NZ,)), dma((NZ, mx)), dma((NZ, mx, mx)), dma((NX, NZ, NY)),
            dma((NZ,)), dma((NZ, mx)), dma((NZ, mx, mx)), dma((NX, NZ, NY)),
            dma((NZ,)), dma((NZ,)), dma((NZ,)), dma((NZ + 1,)),
        ],
        compiler_params=pltpu.CompilerParams(
            collective_id=0, has_side_effects=True, vmem_limit_bytes=64 * 1024 * 1024 - 128 * 1024),
    )(tokens, pre_gain.reshape(1, D), w_expand, w_reduce, post_gain.reshape(1, D))


def solution(mesh):
    return jax.shard_map(
        functools.partial(per_device, mesh.shape["fs"], mesh.shape["tp"]),
        mesh=mesh,
        in_specs=(P(("fs", "tp"), None), P(), P("fs", "tp"), P("tp", "fs"), P()),
        out_specs=P(("fs", "tp"), None),
        check_vma=False,
    )
```

time: 343 us -> 202 us (0.59)
  waiting for transfers between devices: 306 us -> 0 us
  Pallas kernels: 0 us -> 200 us
  matrix products: 16.5 us -> 0 us
  between operations: 13.1 us -> 0.01 us
  other arithmetic: 6.53 us -> 0 us
    all_gather x3 -> x0, waiting for transfers between devices: 274 us -> none  [the longest x1 126 us: per_device(): expand_full = lax.all_gather(w_expand, 'fs', axis=0, tiled=True)]
    pallas_call x0 -> x1, Pallas kernels: none -> 200 us  [per_device(): pl.pallas_call(functools.partial(kernel, NX, NY, NZ), out_shape=jax.Shape...]
    reduce_scatter x1 -> x0, waiting for transfers between devices: 30.1 us -> none  [per_device(): lax.psum_scatter(jnp.dot(hidden, reduce_full, preferred_element_type=jnp....]
    dot_general x1 -> x0, matrix products: 16.5 us -> none  [per_device(): jnp.dot(hidden, reduce_full, preferred_element_type=jnp.float32)]
    convert_element_type x2 -> x0, other arithmetic: 4.05 us -> none  [the longest x1 2.03 us: per_device(): normed = rms_scale(tokens, pre_gain).astype(jnp.bfloat16)]
  transfers between devices with their start and end apart: 4 -> 0, of which waited for: 4 -> 0; matrix products, arithmetic and copies ran while one was open for 0% -> 0% of each run, Pallas kernels for 0% -> 0%
where the time goes in v1:
time: 202 us; the launch traced here: 201 us
  Pallas kernels  200 us (99%)
    pallas_call x1, Pallas kernels, per_device(): pl.pallas_call(functools.partial(kernel, NX, NY, NZ), out_shape=jax.Shape...  200 us

profile of v1, /device:TPU:1, one launch (start us, length us, event | category | flops | bytes accessed | tf_op | source)
XLA Modules:
  0.0 201.5 jit_solution(6358489677507134345)
XLA Ops:
  0.0 199.6 %shard_map.55 = bf16[128,2048]{1,0:T(8,128)(2,1)} custom-call(bf16[128,2048]{1,0:T(8,128)(2,1)} %tok.1, f32[1,2048]{1,0:T(1,128)} %bitcast.2, bf16[256,2048]{1,0:T(8,128)(2,1)} %w_e.1, bf16[2048,256]{1,0:T(8,128)(2,1)} %w_r.1, f32[1,2048]{1,0:T(1,128)} %bitcast.3), custom_call_target="tpu_custom_call" | custom-call | tf_op jit(solution)/shard_map/pallas_call | solution.py:254
  199.6 1.9 copy.7

commit v2 on v1

v2 whole, which is shorter than its diff:
```python
import functools

import jax
import jax.numpy as jnp
from jax import lax
from jax.experimental import pallas as pl
from jax.experimental.pallas import tpu as pltpu
from jax.sharding import PartitionSpec as P

NORM_EPS = 1e-06
MESH = pl.DeviceIdType.MESH


def kernel(NX, NY, NZ, tok, gain_in, w_e, w_r, gain_out, out,
           TG, N, WE, WR, H, O, PR, RX,
           t_ls, t_ps, t_r, e_a, e_b, e_c, e_l, e_r, r_a, r_b, r_c, r_l, r_r, p_s, p_r, c_s, c_r):
    R, D = tok.shape
    DK, F = w_e.shape
    H4 = F // NZ
    fs, tp = lax.axis_index("fs"), lax.axis_index("tp")
    z, y = fs // NY, fs % NY
    x, c = tp // 2, tp % 2
    pc = 1 - c
    peer = (fs, x * 2 + pc)

    def zdev(q):
        return (q * NY + y, tp)

    xs = [(x + j) % NX for j in range(1, NX)]
    ys = [(y + j) % NY for j in range(1, NY)]
    xdevs = [(fs, q * 2 + c) for q in xs]
    ydevs = [(z * NY + q, tp) for q in ys]

    barrier = pltpu.get_barrier_semaphore()
    others = [zdev((z + j) % NZ) for j in range(1, NZ)] + xdevs + ydevs + [peer]
    for dev in others:
        pl.semaphore_signal(barrier, inc=1, device_id=dev, device_id_type=MESH)
    pl.semaphore_wait(barrier, len(others))

    def rc(src, dst, ss, rs, dev):
        return pltpu.make_async_remote_copy(src_ref=src, dst_ref=dst, send_sem=ss, recv_sem=rs,
                                            device_id=dev, device_id_type=MESH)

    sent = []

    def go(cond, make):
        if cond is None:
            make().start()
        else:
            pl.when(cond)(lambda: make().start())
        sent.append((cond, make))

    def guarded(cond, fn):
        if cond is None:
            fn()
        else:
            pl.when(cond)(fn)

    def at_distance(d):
        if d == 0:
            return [(z, 0, None)]
        return [(z - d, -1, z - d >= 0), (z + d, 1, z + d < NZ)]

    def rows_of(start, size, half):
        if half is None:
            return pl.ds(pl.multiple_of(start, size), size)
        return pl.ds(pl.multiple_of(start + half * (size // 2), size // 2), size // 2)

    def e_view(xq, zq, yq, half=None):
        return WE.at[xq, rows_of((zq * NY + yq) * DK, DK, half)]

    def r_view(xq, zq, yq, half=None):
        return WR.at[zq * NY + yq, rows_of(xq * H4, H4, half)]

    def e_piece(q):
        return w_e.at[:, pl.ds(pl.multiple_of(q * H4, H4), H4)]

    def r_piece(q):
        return w_r.at[pl.ds(pl.multiple_of(q * H4, H4), H4)]

    own = [
        pltpu.make_async_copy(tok, TG.at[z, c], t_r.at[z, c]),
        pltpu.make_async_copy(e_piece(z), e_view(x, z, y), e_l.at[z]),
        pltpu.make_async_copy(r_piece(z), r_view(x, z, y), r_l.at[z]),
    ]
    for copy in own:
        copy.start()
    def line_pieces(view, piece, a_s, r):
        for d in range(1, NZ):
            for q, s, ok in at_distance(d):
                go(ok, lambda q=q: rc(piece(q), view(x, z, y), a_s.at[q], r.at[z], zdev(q)))

    def own_tokens():
        for side, (q, ok) in enumerate(((z - 1, z >= 1), (z + 1, z + 1 < NZ))):
            go(ok, lambda q=q, side=side: rc(tok, TG.at[z, c], t_ls.at[z, side], t_r.at[z, c], zdev(q)))
        go(None, lambda: rc(tok, TG.at[z, c], t_ps.at[z], t_r.at[z, c], peer))

    line_pieces(e_view, e_piece, e_a, e_l)
    own_tokens()
    line_pieces(r_view, r_piece, r_a, r_l)

    def landed(ref, sem):
        pltpu.make_async_copy(ref, ref, sem).wait()

    def tokens_step(d):
        for q, s, ok in at_distance(d):
            guarded(ok, lambda q=q: landed(TG.at[q, c], t_r.at[q, c]))
            if d > 0:
                n = z - s
                go(jnp.logical_and(ok, jnp.logical_and(n >= 0, n < NZ)),
                   lambda q=q, n=n, s=s: rc(TG.at[q, c], TG.at[q, c], t_ls.at[q, (1 - s) // 2],
                                            t_r.at[q, c], zdev(n)))
                go(ok, lambda q=q: rc(TG.at[q, c], TG.at[q, c], t_ps.at[q], t_r.at[q, c], peer))

    ways = ((xdevs, xs, ydevs, ys), (ydevs, ys, xdevs, xs))

    def first_step(d, view, l, r, b_s, c_s_):
        for q, s, ok in at_distance(d):
            guarded(ok, lambda q=q: landed(view(x, q, y), l.at[q]))
            for h in (0, 1):
                for j, dev in enumerate(ways[h][0]):
                    go(ok, lambda q=q, j=j, dev=dev, h=h: rc(view(x, q, y, h), view(x, q, y, h), b_s.at[q, j, h],
                                                             r.at[x, q, y, h], dev))
            for h in (0, 1):
                for j, dev in enumerate(ways[h][2]):
                    go(ok, lambda q=q, j=j, dev=dev, h=h: rc(view(x, q, y, h), view(x, q, y, h), c_s_.at[q, 0, j, h],
                                                             r.at[x, q, y, h], dev))

    def second_step(d, view, r, c_s_):
        for q, s, ok in at_distance(d):
            for h in (0, 1):
                for i, m in enumerate(ways[h][1]):
                    where = (m, q, y) if h == 0 else (x, q, m)
                    guarded(ok, lambda where=where, h=h: landed(view(*where, h), r.at[(*where, h)]))
                    for j, dev in enumerate(ways[h][2]):
                        go(ok, lambda q=q, i=i, j=j, dev=dev, where=where, h=h:
                           rc(view(*where, h), view(*where, h), c_s_.at[q, 1 + i, j, h], r.at[(*where, h)], dev))

    def last_step(d, view, r):
        for q, s, ok in at_distance(d):
            for h in (0, 1):
                for a in [x] + xs if h == 0 else xs:
                    for b in ys if h == 0 else [y] + ys:
                        guarded(ok, lambda a=a, b=b, q=q, h=h: landed(view(a, q, b, h), r.at[a, q, b, h]))

    M = 2 * R
    sub = 32

    def rows_step(q):
        landed(TG.at[q, pc], t_r.at[q, pc])

        def norm(i, carry):
            v = TG[q, i // (R // sub), pl.ds(pl.multiple_of((i % (R // sub)) * sub, sub), sub)].astype(jnp.float32)
            v = v * lax.rsqrt(jnp.mean(v * v, axis=-1, keepdims=True) + NORM_EPS) * gain_in[...]
            N[pl.ds(pl.multiple_of(i * sub, sub), sub)] = v.astype(jnp.bfloat16)
            return carry

        lax.fori_loop(0, M // sub, norm, 0)

        def expand(i, carry):
            p = jnp.dot(N[...], WE[i], preferred_element_type=jnp.float32)
            H[i] = jnp.square(jnp.maximum(p, 0.0)).astype(jnp.bfloat16)
            return carry

        lax.fori_loop(0, NX, expand, 0)

        def column(f, carry):
            p = jnp.dot(H[0], WR[f, :H4], preferred_element_type=jnp.float32)
            for xq in range(1, NX):
                p += jnp.dot(H[xq], WR[f, xq * H4:(xq + 1) * H4], preferred_element_type=jnp.float32)
            O[pl.ds(q * 2, 2), f] = p.astype(jnp.bfloat16).reshape(2, R, DK)
            return carry

        lax.fori_loop(0, NZ * NY, column, 0)

    tokens_step(0)
    for d in range(NZ):
        first_step(d, e_view, e_l, e_r, e_b, e_c)
        if d == 0:
            first_step(d, r_view, r_l, r_r, r_b, r_c)
        if d > 0:
            second_step(d - 1, e_view, e_r, e_c)
        if d == NZ - 1:
            tokens_step(1)
    second_step(NZ - 1, e_view, e_r, e_c)
    second_step(0, r_view, r_r, r_c)
    for d in range(1, NZ):
        first_step(d, r_view, r_l, r_r, r_b, r_c)
        if d > 1:
            second_step(d - 1, r_view, r_r, r_c)
            tokens_step(d)
    second_step(NZ - 1, r_view, r_r, r_c)
    for d in range(NZ):
        last_step(d, e_view, e_r)
        last_step(d, r_view, r_r)
    for d in range(NZ):
        for q, s, ok in at_distance(d):
            guarded(ok, lambda q=q: rows_step(q))
            go(ok, lambda q=q: rc(O.at[q * 2 + pc], PR.at[q], p_s.at[q], p_r.at[q], peer))

    def add_block(q, slots):
        def body(f, carry):
            s = O[q * 2 + c, f].astype(jnp.float32) + PR[q, f].astype(jnp.float32)
            for slot in slots:
                s += RX[slot, f].astype(jnp.float32)
            O[q * 2 + c, f] = s.astype(jnp.bfloat16)
            return carry

        lax.fori_loop(0, NZ * NY, body, 0)

    for k in range(NZ):
        landed(PR.at[k], p_r.at[k])

    for j in range(NZ - 1):
        for q, n, ok, has in ((NZ - 1 - j, z + 1, NZ - 1 - j > z, z > 0), (j, z - 1, j < z, z < NZ - 1)):
            inner = jnp.logical_and(ok, has)

            def with_arrived(q=q):
                landed(RX.at[q], c_r.at[q])
                add_block(q, [q])

            pl.when(inner)(with_arrived)
            pl.when(jnp.logical_and(ok, jnp.logical_not(has)))(lambda q=q: add_block(q, []))
            slot = jnp.where(jnp.logical_and(n < z, n == q), NZ, q)
            go(ok, lambda q=q, n=n, slot=slot: rc(O.at[q * 2 + c], RX.at[slot], c_s.at[q], c_r.at[slot], zdev(n)))

    pl.when(z > 0)(lambda: landed(RX.at[z], c_r.at[z]))
    pl.when(z < NZ - 1)(lambda: landed(RX.at[NZ], c_r.at[NZ]))
    pl.when(jnp.logical_and(z > 0, z < NZ - 1))(lambda: add_block(z, [z, NZ]))
    pl.when(z == 0)(lambda: add_block(z, [NZ]))
    pl.when(z == NZ - 1)(lambda: add_block(z, [z]))

    def squares(f, acc):
        m = O[z * 2 + c, f].astype(jnp.float32)
        return acc + jnp.sum(m * m, axis=-1, keepdims=True)

    total = lax.fori_loop(0, NZ * NY, squares, jnp.zeros((R, 1), jnp.float32))
    scale = lax.rsqrt(total / D + NORM_EPS)
    for f in range(NZ * NY):
        cols = slice(f * DK, (f + 1) * DK)
        out[:, cols] = (O[z * 2 + c, f].astype(jnp.float32) * scale * gain_out[:, cols]).astype(jnp.bfloat16)

    for cond, make in sent:
        guarded(cond, lambda make=make: make().wait_send())


def per_device(FS, TP, tokens, pre_gain, w_expand, w_reduce, post_gain):
    NX = TP // 2
    NY = max(k for k in range(1, FS + 1) if FS % k == 0 and (k == 1 or 2 * k * k <= FS))
    NZ = FS // NY
    R, D = tokens.shape
    DK, F = w_expand.shape
    H4 = F // NZ
    bf = jnp.bfloat16
    dma = pltpu.SemaphoreType.DMA
    mx = max(NX, NY)
    vmem = pl.BlockSpec(memory_space=pltpu.VMEM)
    hbm = pl.BlockSpec(memory_space=pl.ANY)
    return pl.pallas_call(
        functools.partial(kernel, NX, NY, NZ),
        out_shape=jax.ShapeDtypeStruct((R, D), bf),
        in_specs=[hbm, vmem, hbm, hbm, vmem],
        out_specs=vmem,
        scratch_shapes=[
            pltpu.VMEM((NZ, 2, R, D), bf),
            pltpu.VMEM((2 * R, D), bf),
            pltpu.VMEM((NX, D, H4), bf),
            pltpu.VMEM((FS, NX * H4, DK), bf),
            pltpu.VMEM((NX, 2 * R, H4), bf),
            pltpu.VMEM((NZ * 2, FS, R, DK), bf),
            pltpu.VMEM((NZ, FS, R, DK), bf),
            pltpu.VMEM((NZ + 1, FS, R, DK), bf),
            dma((NZ, 2)), dma((NZ,)), dma((NZ, 2)),
            dma((NZ,)), dma((NZ, mx, 2)), dma((NZ, mx, mx, 2)), dma((NZ,)), dma((NX, NZ, NY, 2)),
            dma((NZ,)), dma((NZ, mx, 2)), dma((NZ, mx, mx, 2)), dma((NZ,)), dma((NX, NZ, NY, 2)),
            dma((NZ,)), dma((NZ,)), dma((NZ,)), dma((NZ + 1,)),
        ],
        compiler_params=pltpu.CompilerParams(
            collective_id=0, has_side_effects=True, vmem_limit_bytes=64 * 1024 * 1024 - 128 * 1024),
    )(tokens, pre_gain.reshape(1, D), w_expand, w_reduce, post_gain.reshape(1, D))


def solution(mesh):
    return jax.shard_map(
        functools.partial(per_device, mesh.shape["fs"], mesh.shape["tp"]),
        mesh=mesh,
        in_specs=(P(("fs", "tp"), None), P(), P("fs", "tp"), P("tp", "fs"), P()),
        out_specs=P(("fs", "tp"), None),
        check_vma=False,
    )
```

time: 202 us -> 168 us (0.83)
  Pallas kernels: 200 us -> 166 us
    pallas_call x1, Pallas kernels: 200 us -> 166 us  [per_device(): pl.pallas_call(functools.partial(kernel, NX, NY, NZ), out_shape=jax.Shape...]
where the time goes in v2:
time: 168 us
  Pallas kernels  166 us (99%)
  local copies, waits for them, and re-layouts  1.88 us (1%)
    pallas_call x1, Pallas kernels, per_device(): pl.pallas_call(functools.partial(kernel, NX, NY, NZ), out_shape=jax.Shape...  166 us

profile of v2, /device:TPU:1, one launch (start us, length us, event | category | flops | bytes accessed | tf_op | source)
XLA Modules:
  0.0 167.6 jit_solution(295212986904647355)
XLA Ops:
  0.0 165.7 %shard_map.55 = bf16[128,2048]{1,0:T(8,128)(2,1)} custom-call(bf16[128,2048]{1,0:T(8,128)(2,1)} %tok.1, f32[1,2048]{1,0:T(1,128)} %bitcast.2, bf16[256,2048]{1,0:T(8,128)(2,1)} %w_e.1, bf16[2048,256]{1,0:T(8,128)(2,1)} %w_r.1, f32[1,2048]{1,0:T(1,128)} %bitcast.3), custom_call_target="tpu_custom_call" | custom-call | tf_op jit(solution)/shard_map/pallas_call | solution.py:259
  165.8 1.9 %copy.7 = bf16[128,2048]{1,0:T(8,128)(2,1)} copy(bf16[128,2048]{1,0:T(8,128)(2,1)} %shard_map.55) | data formatting | bytes 1048576

commit v3 on v2

--- a/solution.py
+++ b/solution.py
@@ -146,7 +146,7 @@
     M = 2 * R
     sub = 32
 
-    def rows_step(q):
+    def expand_rows(q):
         landed(TG.at[q, pc], t_r.at[q, pc])
 
         def norm(i, carry):
@@ -159,19 +159,24 @@
 
         def expand(i, carry):
             p = jnp.dot(N[...], WE[i], preferred_element_type=jnp.float32)
-            H[i] = jnp.square(jnp.maximum(p, 0.0)).astype(jnp.bfloat16)
+            H[i, pl.ds(pl.multiple_of(q * M, M), M)] = jnp.square(jnp.maximum(p, 0.0)).astype(jnp.bfloat16)
             return carry
 
         lax.fori_loop(0, NX, expand, 0)
 
-        def column(f, carry):
-            p = jnp.dot(H[0], WR[f, :H4], preferred_element_type=jnp.float32)
+    big = 2 * M if NZ % 2 == 0 else M
+
+    def columns(q):
+        def body(k, carry):
+            f, i = q * NY + k // (NZ * M // big), k % (NZ * M // big)
+            row = pl.ds(pl.multiple_of(i * big, big), big)
+            p = jnp.dot(H[0, row], WR[f, :H4], preferred_element_type=jnp.float32)
             for xq in range(1, NX):
-                p += jnp.dot(H[xq], WR[f, xq * H4:(xq + 1) * H4], preferred_element_type=jnp.float32)
-            O[pl.ds(q * 2, 2), f] = p.astype(jnp.bfloat16).reshape(2, R, DK)
+                p += jnp.dot(H[xq, row], WR[f, xq * H4:(xq + 1) * H4], preferred_element_type=jnp.float32)
+            O[pl.ds(i * (big // R), big // R), f] = p.astype(jnp.bfloat16).reshape(big // R, R, DK)
             return carry
 
-        lax.fori_loop(0, NZ * NY, column, 0)
+        lax.fori_loop(0, NY * NZ * M // big, body, 0)
 
     tokens_step(0)
     for d in range(NZ):
@@ -189,16 +194,40 @@
         if d > 1:
             second_step(d - 1, r_view, r_r, r_c)
             tokens_step(d)
-    second_step(NZ - 1, r_view, r_r, r_c)
     for d in range(NZ):
         last_step(d, e_view, e_r)
+
+    def expand_at(d):
+        for q, s, ok in at_distance(d):
+            guarded(ok, lambda q=q: expand_rows(q))
+
+    expand_at(0)
+    expand_at(1)
+    second_step(NZ - 1, r_view, r_r, r_c)
+    for d in range(2, NZ):
+        expand_at(d)
+    for d in range(NZ):
         last_step(d, r_view, r_r)
-    for d in range(NZ):
-        for q, s, ok in at_distance(d):
-            guarded(ok, lambda q=q: rows_step(q))
-            go(ok, lambda q=q: rc(O.at[q * 2 + pc], PR.at[q], p_s.at[q], p_r.at[q], peer))
-
-    def add_block(q, slots):
+        for q, s, ok in at_distance(d):
+            guarded(ok, lambda q=q: columns(q))
+
+    FH = NZ * NY // 2
+
+    def part(h):
+        return pl.ds(h * FH, FH)
+
+    order = []
+    for k in range((NZ + 1) // 2):
+        order += [NZ - 1 - k] + ([k] if k != NZ - 1 - k else [])
+    for h in (0, 1):
+        for q in order:
+            go(None, lambda q=q, h=h: rc(O.at[q * 2 + pc, part(h)], PR.at[q, part(h)], p_s.at[q, h], p_r.at[q, h], peer))
+
+    def add_part(q, h, slots):
+        landed(PR.at[q, part(h)], p_r.at[q, h])
+        for slot in slots:
+            landed(RX.at[slot, part(h)], c_r.at[slot, h])
+
         def body(f, carry):
             s = O[q * 2 + c, f].astype(jnp.float32) + PR[q, f].astype(jnp.float32)
             for slot in slots:
@@ -206,29 +235,20 @@
             O[q * 2 + c, f] = s.astype(jnp.bfloat16)
             return carry
 
-        lax.fori_loop(0, NZ * NY, body, 0)
-
-    for k in range(NZ):
-        landed(PR.at[k], p_r.at[k])
+        lax.fori_loop(h * FH, (h + 1) * FH, body, 0)
 
     for j in range(NZ - 1):
-        for q, n, ok, has in ((NZ - 1 - j, z + 1, NZ - 1 - j > z, z > 0), (j, z - 1, j < z, z < NZ - 1)):
-            inner = jnp.logical_and(ok, has)
-
-            def with_arrived(q=q):
-                landed(RX.at[q], c_r.at[q])
-                add_block(q, [q])
-
-            pl.when(inner)(with_arrived)
-            pl.when(jnp.logical_and(ok, jnp.logical_not(has)))(lambda q=q: add_block(q, []))
-            slot = jnp.where(jnp.logical_and(n < z, n == q), NZ, q)
-            go(ok, lambda q=q, n=n, slot=slot: rc(O.at[q * 2 + c], RX.at[slot], c_s.at[q], c_r.at[slot], zdev(n)))
-
-    pl.when(z > 0)(lambda: landed(RX.at[z], c_r.at[z]))
-    pl.when(z < NZ - 1)(lambda: landed(RX.at[NZ], c_r.at[NZ]))
-    pl.when(jnp.logical_and(z > 0, z < NZ - 1))(lambda: add_block(z, [z, NZ]))
-    pl.when(z == 0)(lambda: add_block(z, [NZ]))
-    pl.when(z == NZ - 1)(lambda: add_block(z, [z]))
+        for h in (0, 1):
+            for q, n, ok, has in ((NZ - 1 - j, z + 1, NZ - 1 - j > z, z > 0), (j, z - 1, j < z, z < NZ - 1)):
+                pl.when(jnp.logical_and(ok, has))(lambda q=q, h=h: add_part(q, h, [q]))
+                pl.when(jnp.logical_and(ok, jnp.logical_not(has)))(lambda q=q, h=h: add_part(q, h, []))
+                slot = jnp.where(jnp.logical_and(n < z, n == q), NZ, q)
+                go(ok, lambda q=q, n=n, slot=slot, h=h: rc(O.at[q * 2 + c, part(h)], RX.at[slot, part(h)],
+                                                           c_s.at[q, h], c_r.at[slot, h], zdev(n)))
+    for h in (0, 1):
+        pl.when(jnp.logical_and(z > 0, z < NZ - 1))(lambda h=h: add_part(z, h, [z, NZ]))
+        pl.when(z == 0)(lambda h=h: add_part(z, h, [NZ]))
+        pl.when(z == NZ - 1)(lambda h=h: add_part(z, h, [z]))
 
     def squares(f, acc):
         m = O[z * 2 + c, f].astype(jnp.float32)
@@ -266,14 +286,14 @@
             pltpu.VMEM((2 * R, D), bf),
             pltpu.VMEM((NX, D, H4), bf),
             pltpu.VMEM((FS, NX * H4, DK), bf),
-            pltpu.VMEM((NX, 2 * R, H4), bf),
+            pltpu.VMEM((NX, NZ * 2 * R, H4), bf),
             pltpu.VMEM((NZ * 2, FS, R, DK), bf),
             pltpu.VMEM((NZ, FS, R, DK), bf),
             pltpu.VMEM((NZ + 1, FS, R, DK), bf),
             dma((NZ, 2)), dma((NZ,)), dma((NZ, 2)),
             dma((NZ,)), dma((NZ, mx, 2)), dma((NZ, mx, mx, 2)), dma((NZ,)), dma((NX, NZ, NY, 2)),
             dma((NZ,)), dma((NZ, mx, 2)), dma((NZ, mx, mx, 2)), dma((NZ,)), dma((NX, NZ, NY, 2)),
-            dma((NZ,)), dma((NZ,)), dma((NZ,)), dma((NZ + 1,)),
+            dma((NZ, 2)), dma((NZ, 2)), dma((NZ, 2)), dma((NZ + 1, 2)),
         ],
         compiler_params=pltpu.CompilerParams(
             collective_id=0, has_side_effects=True, vmem_limit_bytes=64 * 1024 * 1024 - 128 * 1024),

time: 168 us -> 159 us (0.946)
  the two profiles are of different devices: /device:TPU:1 before, /device:TPU:20 now
where the time goes in v3:
time: 159 us; the launch traced here: 158 us
  Pallas kernels  156 us (98%)
  local copies, waits for them, and re-layouts  1.88 us (1%)
    pallas_call x1, Pallas kernels, per_device(): pl.pallas_call(functools.partial(kernel, NX, NY, NZ), out_shape=jax.Shape...  156 us

profile of v3, /device:TPU:20, one launch (start us, length us, event | category | flops | bytes accessed | tf_op | source)
XLA Modules:
  0.0 158.3 jit_solution(6799990072475000852)
XLA Ops:
  0.0 156.4 %shard_map.55 = bf16[128,2048]{1,0:T(8,128)(2,1)} custom-call(bf16[128,2048]{1,0:T(8,128)(2,1)} %tok.1, f32[1,2048]{1,0:T(1,128)} %bitcast.2, bf16[256,2048]{1,0:T(8,128)(2,1)} %w_e.1, bf16[2048,256]{1,0:T(8,128)(2,1)} %w_r.1, f32[1,2048]{1,0:T(1,128)} %bitcast.3), custom_call_target="tpu_custom_call" | custom-call | tf_op jit(solution)/shard_map/pallas_call | solution.py:279
  156.4 1.9 %copy.7 = bf16[128,2048]{1,0:T(8,128)(2,1)} copy(bf16[128,2048]{1,0:T(8,128)(2,1)} %shard_map.55) | data formatting | bytes 1048576
